TPU v7x, 32 devices: a whole 2x2x4 slice. The times are simulated.
32 devices in a mesh: sp: 8 (over z, y), tp: 4 (over x, core).
Axes of the slice: x: 2, y: 2, z: 4, core: 2. Of those that a mesh axis runs over, the one named last changes fastest.
Arguments:
- residual: bfloat16 [1536, 2048], P(('sp', 'tp')), may hold values from -6 to 6
- mixer_input: bfloat16 [1536, 512], P('sp', 'tp'), may hold values from -6 to 6
- log_gate: float32 [1536, 32], P('sp', 'tp'), may hold values from -2 to 0
- decay_rate: float32 [2, 32, 64], P(None, 'tp'), may hold values from 0 to 1
- turn_rate: float32 [2, 32, 64], P(None, 'tp'), may hold values from -1 to 1
- drive_real: float32 [2, 32, 16, 64], P(None, 'tp'), may hold values from -1 to 1
- drive_imaginary: float32 [2, 32, 16, 64], P(None, 'tp'), may hold values from -1 to 1
- read_real: float32 [2, 32, 16, 64], P(None, 'tp'), may hold values from -0.75 to 0.75
- read_imaginary: float32 [2, 32, 16, 64], P(None, 'tp'), may hold values from -0.75 to 0.75
- skip_gain: float32 [512], P('tp'), may hold values from -4 to 4
- project_weight: bfloat16 [512, 2048], replicated, may hold values from -0.25 to 0.25
- norm_gain: float32 [2048], replicated, may hold values from 0.1 to 1.9
- final_gain: float32 [2048], replicated, may hold values from 0.1 to 1.9
- routes: int32 [1536, 2], P('sp'), may hold values from 0 to 7, all different within a row; in each aligned block of 48 rows (0 to 47, 48 to 95, ...) at most 18 rows name the same one
- group_weight: float32 [1536], P('sp'), may hold values from 0.2 to 1
- expert_weight: float32 [1536, 2], P('sp'), may hold values from 0.1 to 1
- gate_weight: bfloat16 [8, 2048, 1024], P('sp', None, 'tp'), may hold values from -0.125 to 0.125
- linear_weight: bfloat16 [8, 2048, 1024], P('sp', None, 'tp'), may hold values from -0.125 to 0.125
- down_weight: bfloat16 [8, 1024, 2048], P('sp', 'tp'), may hold values from -0.1875 to 0.1875
Outputs:
- finished: bfloat16 [1536, 2048], P(('sp', 'tp'))
Inputs may be any that keep to these rules, and one draw needn't show every extreme that they name: `routes`: each row names 2 different experts. In each aligned block of 48 rows no expert is named by more than 18 rows; some expert is named by exactly 18 rows of some block.
All inputs are finite; a program needn't handle non-finite values.
Results may differ from a plain program's by a relative error of at most 0.006.
Values may be sent and summed in bfloat16 or wider, within the bound.
A program may use at most 128 MiB of HBM per device.

v0:
```python
import jax
import jax.numpy as jnp
from jax import lax
from jax.sharding import PartitionSpec as P

deep_alpha = 2.0**0.25
norm_epsilon = 1e-05
highest = lax.Precision.HIGHEST
block_span = 16


def entering_2(part, axis, combine, identity, reverse):
    count = lax.axis_size(axis)
    place = lax.axis_index(axis)
    ahead = count - 1 - place if reverse else place
    gathered = jax.tree.map(lambda a: lax.all_gather(a, axis), part)
    state = jax.tree.map(lambda a, e: jnp.zeros_like(a) + jnp.asarray(e, a.dtype), part, identity)

    def one(step, state):
        source = count - 1 - step if reverse else step
        return combine(
            state, jax.tree.map(lambda a: lax.dynamic_index_in_dim(a, source, 0, False), gathered)
        )

    return lax.fori_loop(0, ahead, one, state)


def layer_norm(values, gain):
    center = values - jnp.mean(values, axis=-1, keepdims=True)
    spread = jnp.mean(center * center, axis=-1, keepdims=True)
    return center * lax.rsqrt(spread + norm_epsilon) * gain


def link_pair(earlier, later):
    decay_real = later[0] * earlier[0] - later[1] * earlier[1]
    decay_imaginary = later[0] * earlier[1] + later[1] * earlier[0]
    state_real = later[0] * earlier[2] - later[1] * earlier[3] + later[2]
    state_imaginary = later[0] * earlier[3] + later[1] * earlier[2] + later[3]
    return (decay_real, decay_imaginary, state_real, state_imaginary)


def block_diagonal(table, groups):
    identity = jnp.eye(groups, dtype=jnp.float32)
    wide = jnp.einsum("ghp,gk->ghkp", table, identity)
    return wide.reshape(table.shape[0] * table.shape[1], groups * table.shape[2])


def direction_terms(inputs, log_gate, rate_row, turn_row, drive_real, drive_imaginary, groups):
    input_scale = jnp.sqrt(1.0 - jnp.exp(-2.0 * rate_row)).reshape(-1)
    push_real = jnp.dot(inputs, block_diagonal(drive_real, groups), precision=highest) * input_scale
    push_imaginary = (
        jnp.dot(inputs, block_diagonal(drive_imaginary, groups), precision=highest) * input_scale
    )
    states_each = rate_row.shape[1]
    widen = jnp.repeat(jnp.eye(groups, dtype=jnp.float32), states_each, axis=1)
    gate_wide = jnp.dot(jnp.exp(log_gate), widen, precision=highest)
    retain = jnp.exp(-rate_row)
    step_real = gate_wide * (retain * jnp.cos(turn_row)).reshape(-1)
    step_imaginary = gate_wide * (retain * jnp.sin(turn_row)).reshape(-1)
    return (step_real, step_imaginary, push_real, push_imaginary)


def local_scan(terms):
    length, width = terms[0].shape
    blocks = length // block_span
    views = [term.reshape(blocks, block_span, width) for term in terms]
    running = tuple((view[:, 0, :] for view in views))
    collected = [running]
    for offset in range(1, block_span):
        running = link_pair(running, tuple((view[:, offset, :] for view in views)))
        collected.append(running)
    within = tuple(
        (jnp.stack([entry[member] for entry in collected], axis=1) for member in range(4))
    )
    totals = tuple((part[:, -1, :] for part in within))
    block_prefix = lax.associative_scan(link_pair, totals, axis=0)
    return (within, block_prefix)


def finish_states(within, block_prefix, carried):
    width = within[0].shape[2]
    ones = jnp.ones((1, width), jnp.float32)
    zeros = jnp.zeros((1, width), jnp.float32)
    starts = (ones, zeros, zeros, zeros)
    exclusive = tuple(
        (
            jnp.concatenate([starts[member], block_prefix[member][:-1]], axis=0)
            for member in range(4)
        )
    )
    entering = link_pair(tuple((part[None, :] for part in carried)), exclusive)
    state_real = (
        within[2] + within[0] * entering[2][:, None, :] - within[1] * entering[3][:, None, :]
    )
    state_imaginary = (
        within[3] + within[0] * entering[3][:, None, :] + within[1] * entering[2][:, None, :]
    )
    return (state_real.reshape(-1, width), state_imaginary.reshape(-1, width))


def read_states(state_real, state_imaginary, read_real, read_imaginary, groups):
    read_table = jnp.concatenate(
        [jnp.transpose(read_real, (0, 2, 1)), -jnp.transpose(read_imaginary, (0, 2, 1))], axis=1
    )
    state_each = read_real.shape[2]
    identity = jnp.eye(groups, dtype=jnp.float32)
    real_part = jnp.einsum("gph,gk->gpkh", read_table[:, :state_each], identity).reshape(
        groups * state_each, -1
    )
    imaginary_part = jnp.einsum("gph,gk->gpkh", read_table[:, state_each:], identity).reshape(
        groups * state_each, -1
    )
    stacked = jnp.concatenate([real_part, imaginary_part], axis=0)
    both = jnp.concatenate([state_real, state_imaginary], axis=1)
    return jnp.dot(both, stacked, precision=highest)


def on_device(
    residual,
    mixer_input,
    log_gate,
    decay_rate,
    turn_rate,
    drive_real,
    drive_imaginary,
    read_real,
    read_imaginary,
    skip_gain,
    project_weight,
    norm_gain,
    final_gain,
    routes,
    group_weight,
    expert_weight,
    gate_weight,
    linear_weight,
    down_weight,
):
    groups = log_gate.shape[1]
    inputs = mixer_input.astype(jnp.float32)
    state_width = groups * decay_rate.shape[2]
    all_ones = jnp.ones((state_width,), jnp.float32)
    all_zeros = jnp.zeros((state_width,), jnp.float32)
    forward = direction_terms(
        inputs, log_gate, decay_rate[0], turn_rate[0], drive_real[0], drive_imaginary[0], groups
    )
    forward_within, forward_prefix = local_scan(forward)
    carry_forward = entering_2(
        (
            forward_prefix[0][-1],
            forward_prefix[1][-1],
            forward_prefix[2][-1],
            forward_prefix[3][-1],
        ),
        "sp",
        link_pair,
        (all_ones, all_zeros, all_zeros, all_zeros),
        False,
    )
    forward_real, forward_imaginary = finish_states(forward_within, forward_prefix, carry_forward)
    backward = direction_terms(
        inputs[::-1],
        log_gate[::-1],
        decay_rate[1],
        turn_rate[1],
        drive_real[1],
        drive_imaginary[1],
        groups,
    )
    backward_within, backward_prefix = local_scan(backward)
    carry_backward = entering_2(
        (
            backward_prefix[0][-1],
            backward_prefix[1][-1],
            backward_prefix[2][-1],
            backward_prefix[3][-1],
        ),
        "sp",
        link_pair,
        (all_ones, all_zeros, all_zeros, all_zeros),
        True,
    )
    backward_real, backward_imaginary = finish_states(
        backward_within, backward_prefix, carry_backward
    )
    readout = read_states(forward_real, forward_imaginary, read_real[0], read_imaginary[0], groups)
    readout = readout + read_states(
        backward_real[::-1], backward_imaginary[::-1], read_real[1], read_imaginary[1], groups
    )
    readout = readout + skip_gain * inputs
    activated = jax.nn.gelu(readout).astype(jnp.bfloat16)
    all_channels = lax.all_to_all(activated, "tp", split_axis=0, concat_axis=1, tiled=True)
    branch = jnp.dot(all_channels, project_weight, preferred_element_type=jnp.float32)
    middle = layer_norm(deep_alpha * residual.astype(jnp.float32) + branch, norm_gain)
    middle_rows = middle.astype(jnp.bfloat16)
    experts = lax.axis_size("sp")
    members = lax.axis_size("tp")
    member = lax.axis_index("tp")
    share_rows, model_width = middle_rows.shape
    top_count = routes.shape[1]
    slot_count = max(2, 3 * share_rows * top_count // (2 * experts))
    chosen = routes.reshape(members, share_rows * top_count)
    matches = (chosen[:, :, None] == jnp.arange(experts, dtype=jnp.int32)[None, None, :]).astype(
        jnp.int32
    )
    order_slot = jnp.sum(jnp.cumsum(matches, axis=1) * matches, axis=2) - 1
    token_index = (
        jnp.arange(members * share_rows * top_count, dtype=jnp.int32).reshape(
            members, share_rows * top_count
        )
        // top_count
    )
    quarter = jnp.broadcast_to(jnp.arange(members, dtype=jnp.int32)[:, None], chosen.shape)
    slot_table = jnp.full((members, experts, slot_count), members * share_rows, jnp.int32)
    slot_table = slot_table.at[quarter, chosen, order_slot].set(token_index)
    zero_row = jnp.zeros((1, model_width), jnp.bfloat16)
    own_table = lax.dynamic_index_in_dim(slot_table, member, 0, keepdims=False)
    local_index = jnp.where(
        own_table < members * share_rows, own_table - member * share_rows, share_rows
    )
    padded = jnp.concatenate([middle_rows, zero_row], axis=0)
    outgoing = padded[local_index]
    landed = lax.all_to_all(outgoing, "sp", split_axis=0, concat_axis=0, tiled=True)
    arrived = lax.all_gather(landed[None], "tp", axis=0, tiled=True)
    expert_input = arrived.reshape(-1, model_width)
    gate_part = jnp.dot(expert_input, gate_weight[0], preferred_element_type=jnp.float32)
    linear_part = jnp.dot(expert_input, linear_weight[0], preferred_element_type=jnp.float32)
    hidden = (jax.nn.silu(gate_part) * linear_part).astype(jnp.bfloat16)
    summed = lax.psum_scatter(
        jnp.dot(hidden, down_weight[0], preferred_element_type=jnp.float32).astype(jnp.bfloat16),
        "tp",
        scatter_dimension=0,
        tiled=True,
    )
    answers = summed.reshape(experts, slot_count, model_width)
    returned = lax.all_to_all(answers, "sp", split_axis=0, concat_axis=0, tiled=True)
    flat_answers = returned.reshape(experts * slot_count, model_width)
    own_routes = lax.dynamic_slice_in_dim(routes, member * share_rows, share_rows, 0)
    own_slots = lax.dynamic_index_in_dim(order_slot, member, 0, keepdims=False).reshape(
        share_rows, top_count
    )
    fetched = flat_answers[own_routes * slot_count + own_slots].astype(jnp.float32)
    mixing = group_weight[:, None] * expert_weight / jnp.sum(expert_weight, axis=1, keepdims=True)
    own_mixing = lax.dynamic_slice_in_dim(mixing, member * share_rows, share_rows, 0)
    routed = jnp.sum(own_mixing[:, :, None] * fetched, axis=1)
    finished = layer_norm(deep_alpha * middle + routed, final_gain)
    return finished.astype(jnp.bfloat16)


def solution(mesh):
    placed = (
        P(("sp", "tp"), None),
        P("sp", "tp"),
        P("sp", "tp"),
        P(None, "tp", None),
        P(None, "tp", None),
        P(None, "tp", None, None),
        P(None, "tp", None, None),
        P(None, "tp", None, None),
        P(None, "tp", None, None),
        P("tp"),
        P(),
        P(),
        P(),
        P("sp", None),
        P("sp"),
        P("sp", None),
        P("sp", None, "tp"),
        P("sp", None, "tp"),
        P("sp", "tp", None),
    )
    return jax.shard_map(
        on_device, mesh=mesh, in_specs=placed, out_specs=P(("sp", "tp"), None), check_vma=False
    )
```

profile of v0, /device:TPU:13, one launch (start us, length us, event | category | flops | bytes accessed | tf_op | source)
XLA Modules:
  0.0 590.7 jit_solution(14900039725470801868)
XLA Ops:
  24.5 2.4 fusion.396
  55.8 2.3 fusion.432
  96.1 19.9 %all-gather.1 = f32[8,1,512]{2,1,0:T(1,128)S(1)} all-gather(f32[1,1,512]{2,1,0:T(1,128)S(1)} %get-tuple-element.749), channel_id=1, replica_groups=mesh['sp'=8,'tp'=4] {'sp'}, dimensions={0}, use_global_device_ids=true | all-gather | bytes 18432 | tf_op jit(solution)/shard_map/all_gather | solution.py:16
  118.7 20.6 %all-gather.2 = f32[8,1,512]{2,1,0:T(1,128)S(1)} all-gather(f32[1,1,512]{2,1,0:T(1,128)S(1)} %add_bitcast_fusion.5), channel_id=1, replica_groups=mesh['sp'=8,'tp'=4] {'sp'}, dimensions={0}, use_global_device_ids=true | all-gather | bytes 18432 | tf_op jit(solution)/shard_map/all_gather | solution.py:16
  142.9 20.6 %all-gather.3 = f32[8,1,512]{2,1,0:T(1,128)S(1)} all-gather(f32[1,1,512]{2,1,0:T(1,128)S(1)} %add_bitcast_fusion.4), channel_id=1, replica_groups=mesh['sp'=8,'tp'=4] {'sp'}, dimensions={0}, use_global_device_ids=true | all-gather | bytes 18432 | tf_op jit(solution)/shard_map/all_gather | solution.py:16
  163.5 20.6 %all-gather.4 = f32[8,1,512]{2,1,0:T(1,128)S(1)} all-gather(f32[1,1,512]{2,1,0:T(1,128)S(1)} %add_bitcast_fusion.3), channel_id=1, replica_groups=mesh['sp'=8,'tp'=4] {'sp'}, dimensions={0}, use_global_device_ids=true | all-gather | bytes 18432 | tf_op jit(solution)/shard_map/all_gather | solution.py:16
  219.8 21.0 %all-gather.5 = f32[8,1,512]{2,1,0:T(1,128)S(1)} all-gather(f32[1,1,512]{2,1,0:T(1,128)} %get-tuple-element.748), channel_id=1, replica_groups=mesh['sp'=8,'tp'=4] {'sp'}, dimensions={0}, use_global_device_ids=true | all-gather | bytes 18432 | tf_op jit(solution)/shard_map/all_gather | solution.py:16
  244.9 21.5 %all-gather.6 = f32[8,1,512]{2,1,0:T(1,128)S(1)} all-gather(f32[1,1,512]{2,1,0:T(1,128)S(1)} %add_bitcast_fusion.2), channel_id=1, replica_groups=mesh['sp'=8,'tp'=4] {'sp'}, dimensions={0}, use_global_device_ids=true | all-gather | bytes 18432 | tf_op jit(solution)/shard_map/all_gather | solution.py:16
  270.7 21.5 %all-gather.7 = f32[8,1,512]{2,1,0:T(1,128)S(1)} all-gather(f32[1,1,512]{2,1,0:T(1,128)S(1)} %add_bitcast_fusion.1), channel_id=1, replica_groups=mesh['sp'=8,'tp'=4] {'sp'}, dimensions={0}, use_global_device_ids=true | all-gather | bytes 18432 | tf_op jit(solution)/shard_map/all_gather | solution.py:16
  292.3 21.5 %all-gather.8 = f32[8,1,512]{2,1,0:T(1,128)S(1)} all-gather(f32[1,1,512]{2,1,0:T(1,128)S(1)} %add_bitcast_fusion), channel_id=1, replica_groups=mesh['sp'=8,'tp'=4] {'sp'}, dimensions={0}, use_global_device_ids=true | all-gather | bytes 18432 | tf_op jit(solution)/shard_map/all_gather | solution.py:16
  335.1 2.3 stack.20
  371.6 2.3 stack.16
  374.0 2.2 multiply_subtract_fusion.1
  378.4 41.4 %all-to-all-start = ((bf16[4,48,128]{2,1,0:T(8,128)(2,1)}), bf16[4,48,128]{2,1,0:T(8,128)(2,1)S(1)}, u32[]{:S(2)}, u32[]{:S(2)}) async-start(bf16[4,48,128]{2,1,0:T(8,128)(2,1)} %bitcast.154), calls=%async_computation | async-start | bytes 98304 | tf_op jit(solution)/shard_map/all_to_all | solution.py:192
  421.0 24.0 %scatter_fusion = s32[4,8,18]{2,1,0:T(8,128)S(1)} fusion(s32[4,8,18]{2,1,0:T(8,128)S(1)} %broadcast_in_dim.19, s32[384]{0:T(512)S(1)} %reshape.461, s32[384]{0:T(512)S(1)} %reshape.463), kind=kCustom, calls=%fused_computation.2 | custom fusion | bytes 9216 | tf_op jit(solution)/shard_map/scatter | solution.py:215
  448.2 25.7 %all_to_all.29 = bf16[8,18,2048]{2,1,0:T(8,128)(2,1)S(1)} all-to-all(bf16[8,18,2048]{2,1,0:T(8,128)(2,1)} %reshape.446), channel_id=1, replica_groups=mesh['sp'=8,'tp'=4] {'sp'}, dimensions={0} | all-to-all | bytes 1179648 | tf_op jit(solution)/shard_map/all_to_all | solution.py:223
  475.1 26.3 %all-gather.11.cloned.1.call-done = bf16[32,18,2048]{2,0,1:T(8,128)(2,1)} async-done(((bf16[8,18,2048]{2,0,1:T(8,128)(2,1)}), bf16[32,18,2048]{2,0,1:T(8,128)(2,1)}) %all-gather.11.cloned.1.call-update) | async-done | bytes 2359312 | tf_op jit(solution)/shard_map/all_gather | solution.py:224
  501.3 4.7 copy.512
  506.1 4.3 reshape.405
  510.4 2.7 fusion.5
  513.1 6.3 %convolution_convert_fusion = bf16[576,2048]{1,0:T(8,128)(2,1)} fusion(bf16[576,2048]{1,0:T(8,128)(2,1)} %reshape.405, bf16[1,256,2048]{2,1,0:T(8,128)(2,1)} %param.41, bf16[1,2048,256]{2,1,0:T(8,128)(2,1)} %param.40, f32[576,256]{1,0:T(8,128)S(1)} %fusion.5), kind=kOutput, calls=%fused_computation.15 | convolution fusion | flops 1210023936 | bytes 7405568 | tf_op jit(solution)/shard_map/dot_general | solution.py:230
  519.4 32.4 %reduce-scatter.2.cloned.1.call-done = bf16[144,2048]{1,0:T(8,128)(2,1)} async-done(((bf16[576,2048]{1,0:T(8,128)(2,1)}), bf16[144,2048]{1,0:T(8,128)(2,1)}) %reduce-scatter.2.cloned.1.call-update) | async-done | bytes 589840 | tf_op jit(solution)/shard_map/reduce_scatter | solution.py:229
  553.9 5.5 all-to-all-start.2
  560.1 16.9 %all-to-all-done.2 = bf16[8,18,2048]{2,1,0:T(8,128)(2,1)} async-done(((bf16[8,18,2048]{2,1,0:T(8,128)(2,1)}), bf16[8,18,2048]{2,1,0:T(8,128)(2,1)}, u32[]{:S(2)}, u32[]{:S(2)}) %all-to-all-start.2) | async-done | bytes 589856 | tf_op jit(solution)/shard_map/all_to_all | solution.py:236
  (840 shorter events, 205.7 us)
Async XLA Ops:
  6.5 438.6 %copy-start = (bf16[512,2048]{1,0:T(8,128)(2,1)S(1)}, bf16[512,2048]{1,0:T(8,128)(2,1)}, u32[]{:S(2)}) copy-start(bf16[512,2048]{1,0:T(8,128)(2,1)} %param.33) | copy-start | bytes 6291460
  60.6 123.6 %copy-start.179 = (f32[2,512]{1,0:T(2,128)}, f32[2,512]{1,0:T(2,128)S(1)}, u32[]{:S(2)}) copy-start(f32[2,512]{1,0:T(2,128)S(1)} %slice.1028) | copy-start | bytes 12292
  61.8 122.3 %copy-start.180 = (f32[2,512]{1,0:T(2,128)}, f32[2,512]{1,0:T(2,128)S(1)}, u32[]{:S(2)}) copy-start(f32[2,512]{1,0:T(2,128)S(1)} %slice.1016) | copy-start | bytes 12292
  68.0 117.3 %copy-start.166 = (f32[2,8,16,64]{3,2,1,0:T(8,128)S(1)}, f32[2,8,16,64]{3,2,1,0:T(8,128)}, u32[]{:S(2)}) copy-start(f32[2,8,16,64]{3,2,1,0:T(8,128)} %param.30) | copy-start | bytes 196612
  78.1 107.2 %copy-start.167 = (f32[2,8,16,64]{3,2,1,0:T(8,128)S(1)}, f32[2,8,16,64]{3,2,1,0:T(8,128)}, u32[]{:S(2)}) copy-start(f32[2,8,16,64]{3,2,1,0:T(8,128)} %param.31) | copy-start | bytes 196612
  192.1 124.8 %copy-start.66 = (f32[12,16,512]{2,0,1:T(8,128)S(1)}, f32[12,16,512]{2,0,1:T(8,128)}, u32[]{:S(2)}) copy-start(f32[12,16,512]{2,0,1:T(8,128)} %constant_dynamic-update-slice_fusion.63) | copy-start | bytes 1179652
  192.1 127.8 %copy-start.37 = (f32[12,1,512]{2,1,0:T(1,128)S(1)}, f32[12,1,512]{2,1,0:T(1,128)}, u32[]{:S(2)}) copy-start(f32[12,1,512]{2,1,0:T(1,128)} %get-tuple-element.494) | copy-start | bytes 73732
  192.1 127.8 %copy-start.39 = (f32[12,1,512]{2,1,0:T(1,128)S(1)}, f32[12,1,512]{2,1,0:T(1,128)}, u32[]{:S(2)}) copy-start(f32[12,1,512]{2,1,0:T(1,128)} %get-tuple-element.478) | copy-start | bytes 73732
  193.0 99.3 %copy-start.193 = (f32[1,512]{1,0:T(1,128)S(1)}, f32[1,512]{1,0:T(1,128)}, u32[]{:S(2)}) copy-start(f32[1,512]{1,0:T(1,128)} %slice.1292) | copy-start | bytes 6148
  193.0 126.2 %copy-start.165 = (f32[12,1,512]{2,0,1:T(8,128)S(1)}, f32[12,1,512]{2,0,1:T(8,128)}, u32[]{:S(2)}) copy-start(f32[12,1,512]{2,0,1:T(8,128)} %get-tuple-element.299) | copy-start | bytes 73732
  193.0 130.8 %copy-start.70 = (f32[12,1,512]{2,0,1:T(8,128)S(1)}, f32[12,1,512]{2,0,1:T(8,128)}, u32[]{:S(2)}) copy-start(f32[12,1,512]{2,0,1:T(8,128)} %get-tuple-element.297) | copy-start | bytes 73732
  193.0 130.8 %copy-start.80 = (f32[12,1,512]{2,0,1:T(8,128)S(1)}, f32[12,1,512]{2,0,1:T(8,128)}, u32[]{:S(2)}) copy-start(f32[12,1,512]{2,0,1:T(8,128)} %get-tuple-element.298) | copy-start | bytes 73732
  193.0 130.9 %copy-start.63 = (f32[12,1,512]{2,1,0:T(1,128)S(1)}, f32[12,1,512]{2,1,0:T(1,128)}, u32[]{:S(2)}) copy-start(f32[12,1,512]{2,1,0:T(1,128)} %get-tuple-element.492) | copy-start | bytes 73732
  193.0 130.9 %copy-start.65 = (f32[12,1,512]{2,1,0:T(1,128)S(1)}, f32[12,1,512]{2,1,0:T(1,128)}, u32[]{:S(2)}) copy-start(f32[12,1,512]{2,1,0:T(1,128)} %get-tuple-element.476) | copy-start | bytes 73732
  199.9 124.0 %copy-start.30 = (f32[12,1,512]{2,1,0:T(1,128)S(1)}, f32[12,1,512]{2,1,0:T(1,128)}, u32[]{:S(2)}) copy-start(f32[12,1,512]{2,1,0:T(1,128)} %get-tuple-element.491) | copy-start | bytes 73732
  199.9 124.0 %copy-start.32 = (f32[12,1,512]{2,1,0:T(1,128)S(1)}, f32[12,1,512]{2,1,0:T(1,128)}, u32[]{:S(2)}) copy-start(f32[12,1,512]{2,1,0:T(1,128)} %get-tuple-element.475) | copy-start | bytes 73732
  206.8 117.1 %copy-start.59 = (f32[12,1,512]{2,1,0:T(1,128)S(1)}, f32[12,1,512]{2,1,0:T(1,128)}, u32[]{:S(2)}) copy-start(f32[12,1,512]{2,1,0:T(1,128)} %get-tuple-element.490) | copy-start | bytes 73732
  206.8 117.1 %copy-start.61 = (f32[12,1,512]{2,1,0:T(1,128)S(1)}, f32[12,1,512]{2,1,0:T(1,128)}, u32[]{:S(2)}) copy-start(f32[12,1,512]{2,1,0:T(1,128)} %get-tuple-element.474) | copy-start | bytes 73732
  214.4 109.6 %copy-start.26 = (f32[12,1,512]{2,1,0:T(1,128)S(1)}, f32[12,1,512]{2,1,0:T(1,128)}, u32[]{:S(2)}) copy-start(f32[12,1,512]{2,1,0:T(1,128)} %get-tuple-element.489) | copy-start | bytes 73732
  214.4 109.6 %copy-start.28 = (f32[12,1,512]{2,1,0:T(1,128)S(1)}, f32[12,1,512]{2,1,0:T(1,128)}, u32[]{:S(2)}) copy-start(f32[12,1,512]{2,1,0:T(1,128)} %get-tuple-element.473) | copy-start | bytes 73732
  378.4 66.7 %all-to-all-start = ((bf16[4,48,128]{2,1,0:T(8,128)(2,1)}), bf16[4,48,128]{2,1,0:T(8,128)(2,1)S(1)}, u32[]{:S(2)}, u32[]{:S(2)}) async-start(bf16[4,48,128]{2,1,0:T(8,128)(2,1)} %bitcast.154), calls=%async_computation | async-start | bytes 98304 | tf_op jit(solution)/shard_map/all_to_all | solution.py:192
  419.9 81.5 %all-gather.11.cloned.1.call-start = ((), (), s32[]{:S(2)}) async-start(), calls=%async_computation.5 | async-start | bytes 2949120 | tf_op jit(solution)/shard_map/all_gather | solution.py:224
  475.0 76.8 %reduce-scatter.2.cloned.1.call-start = ((), (), s32[]{:S(2)}) async-start(), calls=%async_computation.4 | async-start | bytes 2949120 | tf_op jit(solution)/shard_map/reduce_scatter | solution.py:229
  553.9 23.1 %all-to-all-start.2 = ((bf16[8,18,2048]{2,1,0:T(8,128)(2,1)}), bf16[8,18,2048]{2,1,0:T(8,128)(2,1)}, u32[]{:S(2)}, u32[]{:S(2)}) async-start(bf16[8,18,2048]{2,1,0:T(8,128)(2,1)} %reshape.406), calls=%async_computation.3 | async-start | bytes 1572864 | tf_op jit(solution)/shard_map/all_to_all | solution.py:236
  (179 other events, 2777.8 us)
Sparse Core Ops, SparseCore 0:
  475.1 26.1 all-gather.10
  519.5 32.2 reduce-scatter.1
where the time goes:
time: 601 us; the launch traced here: 591 us
  blocking collectives  193 us (32%)
  local copies, waits for them, and re-layouts  176 us (29%)
  waiting for transfers between devices  75.6 us (13%)
  other arithmetic  63.1 us (10%)
  starting transfers between devices  47 us (8%)
  matrix products  19.2 us (3%)
  between operations  16.4 us (3%)
    all_gather x8, blocking collectives, entering_2(): gathered = jax.tree.map(lambda a: lax.all_gather(a, axis), part)  167 us
    unnamed x466, local copies, waits for them, and re-layouts  45.4 us
    all_to_all x1, starting transfers between devices, on_device(): lax.all_to_all(activated, 'tp', split_axis=0, concat_axis=1, tiled=True)  41.4 us
    reduce_scatter x1, waiting for transfers between devices, on_device(): lax.psum_scatter(jnp.dot(hidden, down_weight[0], preferred_element_type=j...  32.4 us
    slice x64, local copies, waits for them, and re-layouts, local_scan(): block_prefix = lax.associative_scan(link_pair, totals, axis=0)  28.5 us
    all_gather x1, waiting for transfers between devices, on_device(): arrived = lax.all_gather(landed[None], 'tp', axis=0, tiled=True)  26.3 us
    all_to_all x1, blocking collectives, on_device(): lax.all_to_all(outgoing, 'sp', split_axis=0, concat_axis=0, tiled=True)  25.7 us
    add x28, local copies, waits for them, and re-layouts, link_pair(): state_real = later[0] * earlier[2] - later[1] * earlier[3] + later[2]  25.4 us
  transfers between devices with their start and end apart: 4, of which 3 were waited for; matrix products, arithmetic and copies ran while one was open for 4% of the time, Pallas kernels for 0%

commit v1 on v0

v1 whole, which is shorter than its diff:
```python
import functools

import jax
import jax.numpy as jnp
from jax import lax
from jax.experimental import pallas as pl
from jax.experimental.pallas import tpu as pltpu
from jax.sharding import PartitionSpec as P

deep_alpha = 2.0**0.25
norm_epsilon = 1e-05
highest = lax.Precision.HIGHEST
f32 = jnp.float32
bf16 = jnp.bfloat16
segments = 8


def layer_norm(values, gain):
    center = values - jnp.mean(values, axis=-1, keepdims=True)
    spread = jnp.mean(center * center, axis=-1, keepdims=True)
    return center * lax.rsqrt(spread + norm_epsilon) * gain


def iota(shape, axis):
    return lax.broadcasted_iota(jnp.int32, shape, axis)


def exact_dot(a, b, dims=((1,), (0,))):
    return lax.dot_general(a, b, (dims, ((), ())), precision=highest, preferred_element_type=f32)


def mixer_kernel(
    n_sp,
    n_tp,
    x_ref,
    gate_ref,
    decay_ref,
    turn_ref,
    drive_re,
    drive_im,
    read_re,
    read_im,
    skip_ref,
    weight_hbm,
    residual_ref,
    gain_ref,
    middle_ref,
    push,
    gate,
    seg,
    enter,
    total,
    totals,
    act,
    chan,
    weight,
    weight_sem,
    send_a,
    recv_a,
    send_b,
    recv_b,
):
    sp = lax.axis_index("sp")
    tp = lax.axis_index("tp")
    barrier = pltpu.get_barrier_semaphore()
    for k in range(1, n_sp):
        pl.semaphore_signal(barrier, inc=1, device_id={"sp": lax.rem(sp + k, n_sp)})
    for k in range(1, n_tp):
        pl.semaphore_signal(barrier, inc=1, device_id={"tp": lax.rem(tp + k, n_tp)})
    fetch = pltpu.make_async_copy(weight_hbm, weight, weight_sem)
    fetch.start()

    length, channels = x_ref.shape
    groups, states = decay_ref.shape[1:]
    width = groups * states
    each = channels // groups
    steps = length // segments
    order = iota((length, length), 0)
    place = iota((length, length), 1)
    shuffle = (place == (order % segments) * steps + order // segments).astype(f32)
    x = jnp.dot(shuffle.astype(bf16), x_ref[...], preferred_element_type=f32)
    spread = (iota((states, width), 1) % states == iota((states, width), 0)).astype(f32)
    own = iota((groups, width), 1) // states == iota((groups, width), 0)
    diagonal = iota((channels, width), 1) // states == iota((channels, width), 0) // each

    def row(values):
        wide = exact_dot(values, spread)
        return jnp.sum(jnp.where(own, wide, 0.0), axis=0, keepdims=True)

    def table(values):
        return jnp.where(diagonal, exact_dot(values, spread), 0.0)

    gate[...] = exact_dot(exact_dot(shuffle, jnp.exp(gate_ref[...])), own.astype(f32))
    turn_rows = []
    for k in range(2):
        rate = decay_ref[k]
        turn = turn_ref[k]
        retain = jnp.exp(-rate)
        scale = row(jnp.sqrt(1.0 - jnp.exp(-2.0 * rate)))
        turn_rows.append((row(retain * jnp.cos(turn)), row(retain * jnp.sin(turn))))
        push[2 * k] = exact_dot(x, table(drive_re[k]) * scale)
        push[2 * k + 1] = exact_dot(x, table(drive_im[k]) * scale)
    (f_re, f_im), (b_re, b_im) = turn_rows

    zero = jnp.zeros((segments, width), f32)
    one = jnp.ones((segments, width), f32)

    def rows_of(j):
        return pl.ds(pl.multiple_of(j * segments, segments), segments)

    def first(j, c):
        out = []
        for k, (sr, si) in enumerate(((f_re, f_im), (b_re, b_im))):
            at = rows_of(j if k == 0 else steps - 1 - j)
            ar, ai, vr, vi = c[4 * k : 4 * k + 4]
            g = gate[at, :]
            mr, mi = g * sr, g * si
            out += [
                mr * ar - mi * ai,
                mr * ai + mi * ar,
                mr * vr - mi * vi + push[2 * k, at, :],
                mr * vi + mi * vr + push[2 * k + 1, at, :],
            ]
        return tuple(out)

    ends = lax.fori_loop(0, steps, first, (one, zero, zero, zero) * 2)
    for i, part in enumerate(ends):
        seg[i] = part

    def link(parts, c):
        ar, ai, vr, vi = parts
        return (ar * c[0] - ai * c[1] + vr, ar * c[1] + ai * c[0] + vi)

    def seg_rows(k, s):
        return [seg[4 * k + i, s : s + 1, :] for i in range(4)]

    for k in range(2):
        span = range(segments) if k == 0 else range(segments - 1, -1, -1)
        decay = (one[:1], zero[:1])
        state = (zero[:1], zero[:1])
        for s in span:
            parts = seg_rows(k, s)
            state = link(parts, state)
            decay = link(parts[:2] + [0.0, 0.0], decay)
        for i, value in enumerate(decay + state):
            total[4 * k + i : 4 * k + i + 1, :] = value
    totals[sp] = total[...]

    pl.semaphore_wait(barrier, n_sp - 1 + n_tp - 1)

    def hand(k):
        peer = lax.rem(sp + k, n_sp)
        return pltpu.make_async_remote_copy(
            src_ref=total,
            dst_ref=totals.at[sp],
            send_sem=send_a.at[k],
            recv_sem=recv_a.at[sp],
            device_id={"sp": peer},
        )

    def arrival(k):
        source = lax.rem(sp + k, n_sp)
        return pltpu.make_async_remote_copy(
            src_ref=total,
            dst_ref=totals.at[source],
            send_sem=send_a.at[k],
            recv_sem=recv_a.at[source],
            device_id={"sp": source},
        )

    for k in range(1, n_sp):
        hand(k).start()
    tables = [(table(read_re[k]), table(read_im[k])) for k in range(2)]
    for k in range(1, n_sp):
        arrival(k).wait_recv()

    for k in range(2):
        c = (zero[:1], zero[:1])
        for d in range(n_sp) if k == 0 else range(n_sp - 1, -1, -1):
            new = link([totals[d, 4 * k + i : 4 * k + i + 1, :] for i in range(4)], c)
            counts = d < sp if k == 0 else d > sp
            c = tuple(jnp.where(counts, a, b) for a, b in zip(new, c))
        for s in range(segments) if k == 0 else range(segments - 1, -1, -1):
            enter[2 * k, s : s + 1, :] = c[0]
            enter[2 * k + 1, s : s + 1, :] = c[1]
            c = link(seg_rows(k, s), c)

    def second(j, c):
        out = []
        for k, (sr, si) in enumerate(((f_re, f_im), (b_re, b_im))):
            at = rows_of(j if k == 0 else steps - 1 - j)
            vr, vi = c[2 * k : 2 * k + 2]
            g = gate[at, :]
            mr, mi = g * sr, g * si
            new_re = mr * vr - mi * vi + push[2 * k, at, :]
            new_im = mr * vi + mi * vr + push[2 * k + 1, at, :]
            push[2 * k, at, :] = new_re
            push[2 * k + 1, at, :] = new_im
            out += [new_re, new_im]
        return tuple(out)

    lax.fori_loop(0, steps, second, tuple(enter[i] for i in range(4)))
    over = ((1,), (1,))
    readout = exact_dot(push[0], tables[0][0], over) - exact_dot(push[1], tables[0][1], over)
    readout = readout + (
        exact_dot(push[2], tables[1][0], over) - exact_dot(push[3], tables[1][1], over)
    )
    readout = readout + skip_ref[...] * x
    mixed = jax.nn.gelu(readout).astype(bf16)
    act[...] = lax.dot_general(
        shuffle.astype(bf16), mixed, (((0,), (0,)), ((), ())), preferred_element_type=f32
    ).astype(bf16)

    share = length // n_tp

    def shift(k, out):
        peer = lax.rem(tp + k, n_tp)
        return pltpu.make_async_remote_copy(
            src_ref=act.at[pl.ds(pl.multiple_of(peer * share, share), share)],
            dst_ref=chan.at[tp if out else peer],
            send_sem=send_b.at[k],
            recv_sem=recv_b.at[tp if out else peer],
            device_id={"tp": peer},
        )

    for k in range(1, n_tp):
        shift(k, True).start()
    chan[tp] = act[pl.ds(pl.multiple_of(tp * share, share), share), :]
    fetch.wait()
    for k in range(1, n_tp):
        shift(k, False).wait_recv()
    whole = jnp.concatenate([chan[m] for m in range(n_tp)], axis=1)
    branch = jnp.dot(whole, weight[...], preferred_element_type=f32)
    middle_ref[...] = layer_norm(
        deep_alpha * residual_ref[...].astype(f32) + branch, gain_ref[...]
    )
    for k in range(1, n_sp):
        hand(k).wait_send()
    for k in range(1, n_tp):
        shift(k, True).wait_send()


def mixer(args, n_sp, n_tp):
    (residual, x, log_gate, decay, turn, d_re, d_im, r_re, r_im, skip, weight, gain) = args
    length, channels = x.shape
    groups, states = decay.shape[1:]
    width = groups * states
    share, model = residual.shape
    flat = lambda a: a.reshape(2, channels, states)
    vmem = pl.BlockSpec(memory_space=pltpu.VMEM)
    dma = pltpu.SemaphoreType.DMA
    return pl.pallas_call(
        functools.partial(mixer_kernel, n_sp, n_tp),
        out_shape=jax.ShapeDtypeStruct((share, model), f32),
        in_specs=[vmem] * 9 + [pl.BlockSpec(memory_space=pl.ANY)] + [vmem] * 2,
        out_specs=vmem,
        scratch_shapes=[
            pltpu.VMEM((4, length, width), f32),
            pltpu.VMEM((length, width), f32),
            pltpu.VMEM((8, segments, width), f32),
            pltpu.VMEM((4, segments, width), f32),
            pltpu.VMEM((8, width), f32),
            pltpu.VMEM((n_sp, 8, width), f32),
            pltpu.VMEM((length, channels), bf16),
            pltpu.VMEM((n_tp, share, channels), bf16),
            pltpu.VMEM(weight.shape, bf16),
            dma(()),
            dma((n_sp,)),
            dma((n_sp,)),
            dma((n_tp,)),
            dma((n_tp,)),
        ],
        compiler_params=pltpu.CompilerParams(
            collective_id=0, has_side_effects=True, vmem_limit_bytes=40 * 2**20
        ),
        name="mixer",
    )(
        x,
        log_gate,
        decay,
        turn,
        flat(d_re),
        flat(d_im),
        flat(r_re),
        flat(r_im),
        skip[None, :],
        weight,
        residual,
        gain[None, :],
    )


def on_device(
    residual,
    mixer_input,
    log_gate,
    decay_rate,
    turn_rate,
    drive_real,
    drive_imaginary,
    read_real,
    read_imaginary,
    skip_gain,
    project_weight,
    norm_gain,
    final_gain,
    routes,
    group_weight,
    expert_weight,
    gate_weight,
    linear_weight,
    down_weight,
):
    experts = lax.axis_size("sp")
    members = lax.axis_size("tp")
    member = lax.axis_index("tp")
    middle = mixer(
        (
            residual,
            mixer_input,
            log_gate,
            decay_rate,
            turn_rate,
            drive_real,
            drive_imaginary,
            read_real,
            read_imaginary,
            skip_gain,
            project_weight,
            norm_gain,
        ),
        experts,
        members,
    )
    middle_rows = middle.astype(bf16)
    share, model = middle.shape
    top = routes.shape[1]
    slots = max(2, 3 * share * top // (2 * experts))
    mixing = group_weight[:, None] * expert_weight / jnp.sum(expert_weight, axis=1, keepdims=True)
    mine = lax.dynamic_slice_in_dim(routes, member * share, share, 0)
    own_mixing = lax.dynamic_slice_in_dim(mixing, member * share, share, 0)
    named = mine[:, :, None] == jnp.arange(experts)[None, None, :]
    uses = jnp.any(named, axis=1)
    earlier = jnp.arange(share)[None, :] < jnp.arange(share)[:, None]
    rank = jnp.dot(earlier.astype(bf16), uses.astype(bf16), preferred_element_type=f32)
    chosen = uses[:, :, None] & (rank[:, :, None] == jnp.arange(slots).astype(f32))
    outgoing = jnp.einsum(
        "nes,nd->esd", chosen.astype(bf16), middle_rows, preferred_element_type=f32
    ).astype(bf16)
    landed = lax.all_to_all(outgoing, "sp", split_axis=0, concat_axis=0, tiled=True)
    arrived = lax.all_gather(landed[None], "tp", axis=0, tiled=True)
    expert_input = arrived.reshape(-1, model)
    gate_part = jnp.dot(expert_input, gate_weight[0], preferred_element_type=f32)
    linear_part = jnp.dot(expert_input, linear_weight[0], preferred_element_type=f32)
    hidden = (jax.nn.silu(gate_part) * linear_part).astype(bf16)
    summed = lax.psum_scatter(
        jnp.dot(hidden, down_weight[0], preferred_element_type=f32).astype(bf16),
        "tp",
        scatter_dimension=0,
        tiled=True,
    )
    answers = summed.reshape(experts, slots, model)
    returned = lax.all_to_all(answers, "sp", split_axis=0, concat_axis=0, tiled=True)
    share_of = jnp.sum(jnp.where(named, own_mixing[:, :, None], 0.0), axis=1)
    weigh = jnp.where(chosen, share_of[:, :, None], 0.0)
    coarse = weigh.astype(bf16)
    fine = (weigh - coarse.astype(f32)).astype(bf16)
    routed = jnp.einsum(
        "nes,esd->nd", jnp.concatenate([coarse, fine]), returned, preferred_element_type=f32
    )
    routed = routed[:share] + routed[share:]
    finished = layer_norm(deep_alpha * middle + routed, final_gain)
    return finished.astype(bf16)


def solution(mesh):
    placed = (
        P(("sp", "tp"), None),
        P("sp", "tp"),
        P("sp", "tp"),
        P(None, "tp", None),
        P(None, "tp", None),
        P(None, "tp", None, None),
        P(None, "tp", None, None),
        P(None, "tp", None, None),
        P(None, "tp", None, None),
        P("tp"),
        P(),
        P(),
        P(),
        P("sp", None),
        P("sp"),
        P("sp", None),
        P("sp", None, "tp"),
        P("sp", None, "tp"),
        P("sp", "tp", None),
    )
    return jax.shard_map(
        on_device, mesh=mesh, in_specs=placed, out_specs=P(("sp", "tp"), None), check_vma=False
    )
```

time: 601 us -> 172 us (0.29)
  the two profiles are of different devices: /device:TPU:13 before, /device:TPU:0 now
where the time goes in v1:
time: 172 us; the launch traced here: 171 us
  waiting for transfers between devices  74.9 us (44%)
  local copies, waits for them, and re-layouts  23.9 us (14%)
  blocking collectives  23.4 us (14%)
  Pallas kernels  18.8 us (11%)
  between operations  13.5 us (8%)
  matrix products  9.26 us (5%)
  starting transfers between devices  5.69 us (3%)
    reduce_scatter x1, waiting for transfers between devices, on_device(): lax.psum_scatter(jnp.dot(hidden, down_weight[0], preferred_element_type=f...  33 us
    all_to_all x1, blocking collectives, on_device(): lax.all_to_all(outgoing, 'sp', split_axis=0, concat_axis=0, tiled=True)  23.4 us
    all_gather x1, waiting for transfers between devices, on_device(): arrived = lax.all_gather(landed[None], 'tp', axis=0, tiled=True)  22.3 us
    all_to_all x1, waiting for transfers between devices, on_device(): lax.all_to_all(answers, 'sp', split_axis=0, concat_axis=0, tiled=True)  19.6 us
    pallas_call x1, Pallas kernels, mixer(): pl.pallas_call(functools.partial(mixer_kernel, n_sp, n_tp), out_shape=jax...  18.8 us
    unnamed x33, local copies, waits for them, and re-layouts  10.6 us
    dot_general x1, matrix products, on_device(): jnp.dot(hidden, down_weight[0], preferred_element_type=f32).astype(bf16)  5.9 us
    all_to_all x1, starting transfers between devices, on_device(): lax.all_to_all(answers, 'sp', split_axis=0, concat_axis=0, tiled=True)  5.65 us
  transfers between devices with their start and end apart: 3, of which 3 were waited for; matrix products, arithmetic and copies ran while one was open for 0% of the time, Pallas kernels for 0%

profile of v1, /device:TPU:0, one launch (start us, length us, event | category | flops | bytes accessed | tf_op | source)
XLA Modules:
  0.0 170.9 jit_solution(5746641567423851535)
XLA Ops:
  6.5 0.9 copy.31.gate_ref
  7.4 0.8 constant_dynamic-slice_fusion
  8.3 1.6 copy-done.1
  9.9 0.9 copy-done.2
  10.9 0.9 copy-done.3
  11.8 0.9 copy-done.4
  12.7 0.9 copy-done.5
  13.6 0.9 copy-done.6
  14.5 0.8 copy-done.7
  15.3 0.7 copy-done.8
  16.0 0.7 copy-done.9
  18.0 18.8 %mixer.1 = f32[48,2048]{1,0:T(8,128)S(1)} custom-call(bf16[192,128]{1,0:T(8,128)(2,1)S(1)} %copy-done.7, f32[192,8]{1,0:T(8,128)S(1)} %copy.31.gate_ref, f32[2,8,64]{2,1,0:T(8,128)S(1)} %copy-done.8, f32[2,8,64]{2,1,0:T(8,128)S(1)} %copy-done.9, f32[2,128,64]{2,1,0:T(8,128)S(1)} %bitcast.25, f32[2,128,64]{2,1,0:T(8,128)S(1)} %bitcast.26, ...), custom_call_target="tpu_custom_call" | custom-call | tf_op jit(solution)/shard_map/mixer/pallas_call | solution.py:252
  37.3 23.4 %all_to_all.10 = bf16[8,18,2048]{2,1,0:T(8,128)(2,1)S(1)} all-to-all(bf16[8,18,2048]{2,1,0:T(8,128)(2,1)S(1)} %convolution_convert_fusion.1), channel_id=1, replica_groups=mesh['sp'=8,'tp'=4] {'sp'}, dimensions={0} | all-to-all | bytes 1179648 | tf_op jit(solution)/shard_map/all_to_all | solution.py:350
  60.7 1.1 copy.32
  61.9 22.3 %all-gather.3.cloned.1.call-done = bf16[32,18,2048]{2,0,1:T(8,128)(2,1)} async-done(((bf16[8,18,2048]{2,0,1:T(8,128)(2,1)}), bf16[32,18,2048]{2,0,1:T(8,128)(2,1)}) %all-gather.3.cloned.1.call-update) | async-done | bytes 2359312 | tf_op jit(solution)/shard_map/all_gather | solution.py:351
  84.2 4.7 %copy.33 = bf16[32,18,2048]{2,1,0:T(8,128)(2,1)} copy(bf16[32,18,2048]{2,0,1:T(8,128)(2,1)} %all-gather.3.cloned.1.call-done) | data formatting | bytes 4718592 | tf_op jit(solution)/shard_map/all_gather | solution.py:351
  88.8 4.4 %reshape.46 = bf16[576,2048]{1,0:T(8,128)(2,1)} reshape(bf16[32,18,2048]{2,1,0:T(8,128)(2,1)} %copy.33) | data formatting | bytes 4718592 | tf_op jit(solution)/shard_map/reshape | solution.py:352
  93.3 2.5 %fusion.4 = f32[576,256]{1,0:T(8,128)S(1)} fusion(bf16[576,2048]{1,0:T(8,128)(2,1)} %reshape.46, bf16[1,2048,256]{2,1,0:T(8,128)(2,1)S(1)} %copy-done.14), kind=kOutput, calls=%fused_computation.7 | convolution fusion | flops 603979776 | bytes 3997696 | tf_op jit(solution)/shard_map/dot_general | solution.py:353
  95.7 5.9 %convolution_convert_fusion = bf16[576,2048]{1,0:T(8,128)(2,1)} fusion(bf16[576,2048]{1,0:T(8,128)(2,1)} %reshape.46, bf16[1,256,2048]{2,1,0:T(8,128)(2,1)S(1)} %copy-done, bf16[1,2048,256]{2,1,0:T(8,128)(2,1)} %param.36, f32[576,256]{1,0:T(8,128)S(1)} %fusion.4), kind=kOutput, calls=%fused_computation | convolution fusion | flops 1210023936 | bytes 7405568 | tf_op jit(solution)/shard_map/dot_general | solution.py:357
  101.7 33.0 %reduce-scatter.2.cloned.1.call-done = bf16[144,2048]{1,0:T(8,128)(2,1)} async-done(((bf16[576,2048]{1,0:T(8,128)(2,1)}), bf16[144,2048]{1,0:T(8,128)(2,1)}) %reduce-scatter.2.cloned.1.call-update) | async-done | bytes 589840 | tf_op jit(solution)/shard_map/reduce_scatter | solution.py:356
  134.6 2.1 %reshape.47 = bf16[8,18,2048]{2,1,0:T(8,128)(2,1)} reshape(bf16[144,2048]{1,0:T(8,128)(2,1)} %reduce-scatter.2.cloned.1.call-done) | data formatting | bytes 1179648 | tf_op jit(solution)/shard_map/reshape | solution.py:362
  136.8 5.6 %all-to-all-start.1 = ((bf16[8,18,2048]{2,1,0:T(8,128)(2,1)}), bf16[8,18,2048]{2,1,0:T(8,128)(2,1)S(1)}, u32[]{:S(2)}, u32[]{:S(2)}) async-start(bf16[8,18,2048]{2,1,0:T(8,128)(2,1)} %reshape.47), calls=%async_computation.2 | async-start | bytes 1572864 | tf_op jit(solution)/shard_map/all_to_all | solution.py:363
  142.9 19.6 %all-to-all-done.1 = bf16[8,18,2048]{2,1,0:T(8,128)(2,1)S(1)} async-done(((bf16[8,18,2048]{2,1,0:T(8,128)(2,1)}), bf16[8,18,2048]{2,1,0:T(8,128)(2,1)S(1)}, u32[]{:S(2)}, u32[]{:S(2)}) %all-to-all-start.1) | async-done | bytes 589856 | tf_op jit(solution)/shard_map/all_to_all | solution.py:363
  163.3 0.8 multiply_convert_fusion
  (43 shorter events, 3.2 us)
Async XLA Ops:
  6.5 89.2 %copy-start = (bf16[1,256,2048]{2,1,0:T(8,128)(2,1)S(1)}, bf16[1,256,2048]{2,1,0:T(8,128)(2,1)}, u32[]{:S(2)}) copy-start(bf16[1,256,2048]{2,1,0:T(8,128)(2,1)} %param.37) | copy-start | bytes 3145732
  6.5 77.6 %all-gather.3.cloned.1.call-start = ((), (), s32[]{:S(2)}) async-start(), calls=%async_computation.4 | async-start | bytes 2949120 | tf_op jit(solution)/shard_map/all_gather | solution.py:351
  8.3 1.6 copy-start.1
  9.9 0.9 copy-start.2
  10.9 0.9 copy-start.3
  11.8 0.9 copy-start.4
  12.7 0.9 copy-start.5
  13.6 0.9 copy-start.6
  14.5 0.8 copy-start.7
  15.3 0.7 copy-start.8
  16.0 0.7 copy-start.9
  16.7 0.7 copy-start.10
  17.4 0.7 copy-start.11
  61.8 72.8 %reduce-scatter.2.cloned.1.call-start = ((), (), s32[]{:S(2)}) async-start(), calls=%async_computation.3 | async-start | bytes 2949120 | tf_op jit(solution)/shard_map/reduce_scatter | solution.py:356
  88.8 4.4 %copy-start.14 = (bf16[1,2048,256]{2,1,0:T(8,128)(2,1)S(1)}, bf16[1,2048,256]{2,1,0:T(8,128)(2,1)}, u32[]{:S(2)}) copy-start(bf16[1,2048,256]{2,1,0:T(8,128)(2,1)} %param.35) | copy-start | bytes 3145732
  101.6 40.8 %copy-start.13 = (f32[192,2]{0,1:T(2,128)S(1)}, f32[192,2]{0,1:T(2,128)}, u32[]{:S(2)}) copy-start(f32[192,2]{0,1:T(2,128)} %param.34) | copy-start | bytes 4612
  101.6 40.9 %copy-start.15 = (f32[192]{0:T(256)S(1)}, f32[192]{0:T(256)}, u32[]{:S(2)}) copy-start(f32[192]{0:T(256)} %param.33) | copy-start | bytes 2308
  136.8 26.5 %copy-start.12 = (f32[2048]{0:T(1024)S(1)}, f32[2048]{0:T(1024)}, u32[]{:S(2)}) copy-start(f32[2048]{0:T(1024)} %param.31) | copy-start | bytes 24580
  136.8 25.7 %all-to-all-start.1 = ((bf16[8,18,2048]{2,1,0:T(8,128)(2,1)}), bf16[8,18,2048]{2,1,0:T(8,128)(2,1)S(1)}, u32[]{:S(2)}, u32[]{:S(2)}) async-start(bf16[8,18,2048]{2,1,0:T(8,128)(2,1)} %reshape.47), calls=%async_computation.2 | async-start | bytes 1572864 | tf_op jit(solution)/shard_map/all_to_all | solution.py:363
Sparse Core Ops, SparseCore 0:
  62.0 22.1 all-gather.2
  101.8 32.8 reduce-scatter.1

commit v2 on v1

--- a/solution.py
+++ b/solution.py
@@ -290,6 +290,254 @@
     )
 
 
+def experts_kernel(
+    n_sp,
+    n_tp,
+    middle_ref,
+    meta_ref,
+    gain_ref,
+    gate_hbm,
+    linear_hbm,
+    down_hbm,
+    out_ref,
+    rows_out,
+    recv,
+    part,
+    sib,
+    pair,
+    peer_sum,
+    final,
+    back,
+    gate_w,
+    linear_w,
+    down_w,
+    weight_sems,
+    s1,
+    r1,
+    s2x,
+    s2d,
+    r2,
+    s3,
+    r3,
+    s4,
+    r4,
+    s5,
+    r5,
+):
+    sp = lax.axis_index("sp")
+    tp = lax.axis_index("tp")
+    n_hi = n_tp // 2
+    hi = tp // 2
+    lo = tp % 2
+    sibling = hi * 2 + 1 - lo
+    barrier = pltpu.get_barrier_semaphore()
+    for k in range(1, n_sp):
+        pl.semaphore_signal(barrier, inc=1, device_id={"sp": lax.rem(sp + k, n_sp)})
+    for k in range(1, n_tp):
+        pl.semaphore_signal(barrier, inc=1, device_id={"tp": lax.rem(tp + k, n_tp)})
+    fetches = [
+        pltpu.make_async_copy(gate_hbm.at[0], gate_w, weight_sems.at[0]),
+        pltpu.make_async_copy(linear_hbm.at[0], linear_w, weight_sems.at[1]),
+        pltpu.make_async_copy(down_hbm.at[0], down_w, weight_sems.at[2]),
+    ]
+    for fetch in fetches:
+        fetch.start()
+
+    share, model = middle_ref.shape
+    length = meta_ref.shape[0]
+    slots = rows_out.shape[1]
+    pick = (iota((length, share), 0) == tp * share + iota((length, share), 1)).astype(f32)
+    facts = exact_dot(meta_ref[...], pick, ((0,), (0,)))
+    expert = iota((n_sp, share), 0).astype(f32)
+    first, second = facts[0:1] == expert, facts[1:2] == expert
+    uses = jnp.where(first, 1.0, 0.0) + jnp.where(second, 1.0, 0.0)
+    weights = jnp.where(first, facts[2:3], 0.0) + jnp.where(second, facts[3:4], 0.0)
+    before = (iota((share, share), 0) < iota((share, share), 1)).astype(bf16)
+    rank = jnp.dot(uses.astype(bf16), before, preferred_element_type=f32)
+    slot = iota((slots, share), 0).astype(f32)
+    chosen = [
+        jnp.where(slot == rank[e : e + 1], uses[e : e + 1], 0.0) for e in range(n_sp)
+    ]
+    weigh = jnp.concatenate([chosen[e] * weights[e : e + 1] for e in range(n_sp)], axis=0)
+    chosen = jnp.concatenate(chosen, axis=0).astype(bf16)
+    rows = jnp.dot(chosen, middle_ref[...].astype(bf16), preferred_element_type=f32)
+    for e in range(n_sp):
+        rows_out[e] = rows[e * slots : (e + 1) * slots].astype(bf16)
+
+    pl.semaphore_wait(barrier, n_sp - 1 + n_tp - 1)
+
+    def remote(src, dst, send, receive, where):
+        return pltpu.make_async_remote_copy(
+            src_ref=src, dst_ref=dst, send_sem=send, recv_sem=receive, device_id=where
+        )
+
+    def plus(k):
+        return lax.rem(sp + k, n_sp)
+
+    def minus(k):
+        return lax.rem(sp + n_sp - k, n_sp)
+
+    def up(k):
+        return lax.rem(hi + k, n_hi)
+
+    sends = []
+
+    def go(copy):
+        copy.start()
+        sends.append(copy)
+
+    for k in range(1, n_sp):
+        e = plus(k)
+        go(remote(rows_out.at[e], recv.at[tp, sp], s1.at[k], r1.at[sp], {"sp": e}))
+    recv[tp, sp] = rows_out[sp]
+
+    def landed(m, s, sem):
+        remote(rows_out.at[0], recv.at[m, s], s1.at[0], sem, {"sp": plus(1)}).wait_recv()
+
+    def to_sibling(h, s):
+        block = recv.at[h * 2 + lo, s]
+        go(remote(block, block, s2d.at[h, s], r2.at[h * 2 + lo, s], {"tp": sibling}))
+
+    def pass_own(s):
+        for k in range(1, n_hi):
+            h = up(k)
+            block = recv.at[tp, s]
+            go(remote(block, block, s2x.at[h, s], r2.at[tp, s], {"tp": h * 2 + lo}))
+        to_sibling(hi, s)
+
+    pass_own(sp)
+    for k in range(1, n_sp):
+        s = minus(k)
+        landed(tp, s, r1.at[s])
+        pass_own(s)
+    for k in range(1, n_hi):
+        h = up(k)
+        for j in range(n_sp):
+            s = minus(j)
+            landed(h * 2 + lo, s, r2.at[h * 2 + lo, s])
+            to_sibling(h, s)
+    for fetch in fetches:
+        fetch.wait()
+
+    def flat(block):
+        return block.astype(f32).reshape(n_sp * slots, model).astype(bf16)
+
+    def compute(g):
+        x = flat(recv[g])
+        a = jnp.dot(x, gate_w[...], preferred_element_type=f32)
+        b = jnp.dot(x, linear_w[...], preferred_element_type=f32)
+        hidden = (jax.nn.silu(a) * b).astype(bf16)
+        y = jnp.dot(hidden, down_w[...], preferred_element_type=f32)
+        part[g] = y.reshape(n_sp, slots, model).astype(bf16)
+
+    def give(h):
+        go(remote(part.at[h * 2 + 1 - lo], sib.at[h], s3.at[h], r3.at[h], {"tp": sibling}))
+
+    def given(h):
+        remote(part.at[0], sib.at[h], s3.at[h], r3.at[h], {"tp": sibling}).wait_recv()
+
+    compute(tp)
+    for j in range(n_sp):
+        s = minus(j)
+        landed(sibling, s, r2.at[sibling, s])
+    compute(sibling)
+    give(hi)
+    for k in range(1, n_hi):
+        h = up(k)
+        other = h * 2 + 1 - lo
+        for j in range(n_sp):
+            s = minus(j)
+            landed(other, s, r2.at[other, s])
+        compute(other)
+        give(h)
+        compute(h * 2 + lo)
+        given(h)
+        for j in range(n_sp):
+            s = plus(j)
+            pair[h, s] = (part[h * 2 + lo, s].astype(f32) + sib[h, s].astype(f32)).astype(bf16)
+            go(
+                remote(
+                    pair.at[h, s],
+                    peer_sum.at[hi, s],
+                    s4.at[h, s],
+                    r4.at[hi, s],
+                    {"tp": h * 2 + lo},
+                )
+            )
+    given(hi)
+    for j in range(n_sp):
+        s = plus(j)
+        value = part[tp, s].astype(f32) + sib[hi, s].astype(f32)
+        for k in range(1, n_hi):
+            h = up(k)
+            remote(
+                pair.at[0, 0], peer_sum.at[h, s], s4.at[0, 0], r4.at[h, s], {"tp": sibling}
+            ).wait_recv()
+            value = value + peer_sum[h, s].astype(f32)
+        if j == 0:
+            back[sp] = value.astype(bf16)
+        else:
+            final[s] = value.astype(bf16)
+            go(remote(final.at[s], back.at[sp], s5.at[j], r5.at[sp], {"sp": s}))
+    coarse = weigh.astype(bf16)
+    fine = (weigh - coarse.astype(f32)).astype(bf16)
+    for j in range(1, n_sp):
+        s = minus(j)
+        remote(final.at[0], back.at[s], s5.at[0], r5.at[s], {"sp": plus(1)}).wait_recv()
+    answers = flat(back[...])
+    over = (((0,), (0,)), ((), ()))
+    routed = lax.dot_general(coarse, answers, over, preferred_element_type=f32)
+    routed = routed + lax.dot_general(fine, answers, over, preferred_element_type=f32)
+    out_ref[...] = layer_norm(deep_alpha * middle_ref[...] + routed, gain_ref[...]).astype(bf16)
+    for copy in sends:
+        copy.wait_send()
+
+
+def experts_layer(middle, meta, gain, gate_weight, linear_weight, down_weight, n_sp, n_tp, slots):
+    share, model = middle.shape
+    hidden = gate_weight.shape[2]
+    n_hi = n_tp // 2
+    vmem = pl.BlockSpec(memory_space=pltpu.VMEM)
+    hbm = pl.BlockSpec(memory_space=pl.ANY)
+    dma = pltpu.SemaphoreType.DMA
+    block = (n_sp, slots, model)
+    return pl.pallas_call(
+        functools.partial(experts_kernel, n_sp, n_tp),
+        out_shape=jax.ShapeDtypeStruct((share, model), bf16),
+        in_specs=[vmem] * 3 + [hbm] * 3,
+        out_specs=vmem,
+        scratch_shapes=[
+            pltpu.VMEM(block, bf16),
+            pltpu.VMEM((n_tp,) + block, bf16),
+            pltpu.VMEM((n_tp,) + block, bf16),
+            pltpu.VMEM((n_hi,) + block, bf16),
+            pltpu.VMEM((n_hi,) + block, bf16),
+            pltpu.VMEM((n_hi,) + block, bf16),
+            pltpu.VMEM(block, bf16),
+            pltpu.VMEM(block, bf16),
+            pltpu.VMEM((model, hidden), bf16),
+            pltpu.VMEM((model, hidden), bf16),
+            pltpu.VMEM((hidden, model), bf16),
+            dma((3,)),
+            dma((n_sp,)),
+            dma((n_sp,)),
+            dma((n_hi, n_sp)),
+            dma((n_hi, n_sp)),
+            dma((n_tp, n_sp)),
+            dma((n_hi,)),
+            dma((n_hi,)),
+            dma((n_hi, n_sp)),
+            dma((n_hi, n_sp)),
+            dma((n_sp,)),
+            dma((n_sp,)),
+        ],
+        compiler_params=pltpu.CompilerParams(
+            collective_id=1, has_side_effects=True, vmem_limit_bytes=60 * 2**20
+        ),
+        name="experts",
+    )(middle, meta, gain[None, :], gate_weight, linear_weight, down_weight)
+
+
 def on_device(
     residual,
     mixer_input,
@@ -313,7 +561,6 @@
 ):
     experts = lax.axis_size("sp")
     members = lax.axis_size("tp")
-    member = lax.axis_index("tp")
     middle = mixer(
         (
             residual,
@@ -332,45 +579,23 @@
         experts,
         members,
     )
-    middle_rows = middle.astype(bf16)
-    share, model = middle.shape
+    share = residual.shape[0]
     top = routes.shape[1]
     slots = max(2, 3 * share * top // (2 * experts))
+    slots = -(-slots // 8) * 8
     mixing = group_weight[:, None] * expert_weight / jnp.sum(expert_weight, axis=1, keepdims=True)
-    mine = lax.dynamic_slice_in_dim(routes, member * share, share, 0)
-    own_mixing = lax.dynamic_slice_in_dim(mixing, member * share, share, 0)
-    named = mine[:, :, None] == jnp.arange(experts)[None, None, :]
-    uses = jnp.any(named, axis=1)
-    earlier = jnp.arange(share)[None, :] < jnp.arange(share)[:, None]
-    rank = jnp.dot(earlier.astype(bf16), uses.astype(bf16), preferred_element_type=f32)
-    chosen = uses[:, :, None] & (rank[:, :, None] == jnp.arange(slots).astype(f32))
-    outgoing = jnp.einsum(
-        "nes,nd->esd", chosen.astype(bf16), middle_rows, preferred_element_type=f32
-    ).astype(bf16)
-    landed = lax.all_to_all(outgoing, "sp", split_axis=0, concat_axis=0, tiled=True)
-    arrived = lax.all_gather(landed[None], "tp", axis=0, tiled=True)
-    expert_input = arrived.reshape(-1, model)
-    gate_part = jnp.dot(expert_input, gate_weight[0], preferred_element_type=f32)
-    linear_part = jnp.dot(expert_input, linear_weight[0], preferred_element_type=f32)
-    hidden = (jax.nn.silu(gate_part) * linear_part).astype(bf16)
-    summed = lax.psum_scatter(
-        jnp.dot(hidden, down_weight[0], preferred_element_type=f32).astype(bf16),
-        "tp",
-        scatter_dimension=0,
-        tiled=True,
+    meta = jnp.concatenate([routes.astype(f32), mixing], axis=1)
+    return experts_layer(
+        middle,
+        meta,
+        final_gain,
+        gate_weight,
+        linear_weight,
+        down_weight,
+        experts,
+        members,
+        slots,
     )
-    answers = summed.reshape(experts, slots, model)
-    returned = lax.all_to_all(answers, "sp", split_axis=0, concat_axis=0, tiled=True)
-    share_of = jnp.sum(jnp.where(named, own_mixing[:, :, None], 0.0), axis=1)
-    weigh = jnp.where(chosen, share_of[:, :, None], 0.0)
-    coarse = weigh.astype(bf16)
-    fine = (weigh - coarse.astype(f32)).astype(bf16)
-    routed = jnp.einsum(
-        "nes,esd->nd", jnp.concatenate([coarse, fine]), returned, preferred_element_type=f32
-    )
-    routed = routed[:share] + routed[share:]
-    finished = layer_norm(deep_alpha * middle + routed, final_gain)
-    return finished.astype(bf16)
 
 
 def solution(mesh):

time: 172 us -> 95.9 us (0.56)
  the two profiles are of different devices: /device:TPU:0 before, /device:TPU:13 now
where the time goes in v2:
time: 95.9 us; the launch traced here: 95.3 us
  Pallas kernels  79.6 us (83%)
  local copies, waits for them, and re-layouts  13.6 us (14%)
  other arithmetic  2.1 us (2%)
    pallas_call x1, Pallas kernels, experts_layer(): pl.pallas_call(functools.partial(experts_kernel, n_sp, n_tp), out_shape=j...  63.2 us
    pallas_call x1, Pallas kernels, mixer(): pl.pallas_call(functools.partial(mixer_kernel, n_sp, n_tp), out_shape=jax...  16.4 us
    unnamed x26, local copies, waits for them, and re-layouts  12.8 us

profile of v2, /device:TPU:13, one launch (start us, length us, event | category | flops | bytes accessed | tf_op | source)
XLA Modules:
  0.0 95.3 jit_solution(2752798548873979199)
XLA Ops:
  0.0 0.7 reduce_sum.9
  0.7 0.7 multiply_divide_fusion
  1.4 0.7 convert_element_type.3
  2.1 0.8 copy.26.meta_ref
  2.9 0.8 copy.25.gate_ref
  3.7 0.0 copy-start
  3.7 1.6 %copy-done = bf16[512,2048]{1,0:T(8,128)(2,1)S(1)} copy-done((bf16[512,2048]{1,0:T(8,128)(2,1)S(1)}, bf16[512,2048]{1,0:T(8,128)(2,1)}, u32[]{:S(2)}) %copy-start) | copy-done | bytes 2097176
  5.3 0.0 copy-start.2
  5.3 0.9 copy-done.2
  6.2 0.0 copy-start.3
  6.2 0.9 copy-done.3
  7.1 0.9 copy-done.4
  8.0 0.9 copy-done.5
  8.9 0.9 copy-done.6
  9.8 0.8 copy-done.7
  10.6 0.7 copy-done.8
  11.3 0.7 copy-done.9
  12.0 0.7 copy-done.10
  12.7 0.7 copy-done.11
  13.4 16.4 %mixer.1.middle_ref = f32[48,2048]{1,0:T(8,128)S(1)} custom-call(bf16[192,128]{1,0:T(8,128)(2,1)S(1)} %copy-done.7, f32[192,8]{1,0:T(8,128)S(1)} %copy.25.gate_ref, f32[2,8,64]{2,1,0:T(8,128)S(1)} %copy-done.8, f32[2,8,64]{2,1,0:T(8,128)S(1)} %copy-done.9, f32[2,128,64]{2,1,0:T(8,128)S(1)} %bitcast.7, f32[2,128,64]{2,1,0:T(8,128)S(1)} %bitcast.8, ...), custom_call_target="tpu_custom_call" | custom-call | tf_op jit(solution)/shard_map/mixer/pallas_call | solution.py:252
  29.8 0.0 copy-start.1
  29.8 0.7 copy-done.1
  30.5 63.2 %experts.1 = bf16[48,2048]{1,0:T(8,128)(2,1)} custom-call(f32[48,2048]{1,0:T(8,128)} %copy-done.1, f32[192,4]{1,0:T(8,128)} %copy.26.meta_ref, f32[1,2048]{1,0:T(1,128)} %bitcast.13, bf16[1,2048,256]{2,1,0:T(8,128)(2,1)} %gate_hbm.1, bf16[1,2048,256]{2,1,0:T(8,128)(2,1)} %linear_hbm.1, bf16[1,256,2048]{2,1,0:T(8,128)(2,1)} %down_hbm.1), custom_call_target="tpu_custom_call" | custom-call | tf_op jit(solution)/shard_map/experts/pallas_call | solution.py:504
  93.7 1.6 %copy.28 = bf16[48,2048]{1,0:T(8,128)(2,1)} copy(bf16[48,2048]{1,0:T(8,128)(2,1)} %experts.1) | data formatting | bytes 393216
  (9 shorter events, 0.0 us)
Async XLA Ops:
  3.7 1.6 %copy-start = (bf16[512,2048]{1,0:T(8,128)(2,1)S(1)}, bf16[512,2048]{1,0:T(8,128)(2,1)}, u32[]{:S(2)}) copy-start(bf16[512,2048]{1,0:T(8,128)(2,1)} %weight_hbm.1) | copy-start | bytes 6291460
  5.3 0.9 copy-start.2
  6.2 0.9 copy-start.3
  7.1 0.9 copy-start.4
  8.0 0.9 copy-start.5
  8.9 0.9 copy-start.6
  9.8 0.8 copy-start.7
  10.6 0.7 copy-start.8
  11.3 0.7 copy-start.9
  12.0 0.7 copy-start.10
  12.7 0.7 copy-start.11
  29.8 0.7 copy-start.1

commit v3 on v2

--- a/solution.py
+++ b/solution.py
@@ -29,37 +29,18 @@
     return lax.dot_general(a, b, (dims, ((), ())), precision=highest, preferred_element_type=f32)
 
 
-def mixer_kernel(
-    n_sp,
-    n_tp,
-    x_ref,
-    gate_ref,
-    decay_ref,
-    turn_ref,
-    drive_re,
-    drive_im,
-    read_re,
-    read_im,
-    skip_ref,
-    weight_hbm,
-    residual_ref,
-    gain_ref,
-    middle_ref,
-    push,
-    gate,
-    seg,
-    enter,
-    total,
-    totals,
-    act,
-    chan,
-    weight,
-    weight_sem,
-    send_a,
-    recv_a,
-    send_b,
-    recv_b,
-):
+def mixer_kernel(n_sp, n_tp, *refs):
+    sources, middle_ref, staged = refs[:12], refs[12], refs[13:25]
+    (push, gate, seg, enter, total, totals, act, chan) = refs[25:33]
+    (stage_sems, send_a, recv_a, send_b, recv_b) = refs[33:]
+    loads = [
+        pltpu.make_async_copy(source, place, stage_sems.at[i])
+        for i, (source, place) in enumerate(zip(sources, staged))
+    ]
+    for load in loads:
+        load.start()
+    (x_ref, gate_ref, decay_ref, turn_ref, drive_re, drive_im) = staged[:6]
+    (read_re, read_im, skip_ref, residual_ref, gain_ref, weight) = staged[6:]
     sp = lax.axis_index("sp")
     tp = lax.axis_index("tp")
     barrier = pltpu.get_barrier_semaphore()
@@ -67,8 +48,8 @@
         pl.semaphore_signal(barrier, inc=1, device_id={"sp": lax.rem(sp + k, n_sp)})
     for k in range(1, n_tp):
         pl.semaphore_signal(barrier, inc=1, device_id={"tp": lax.rem(tp + k, n_tp)})
-    fetch = pltpu.make_async_copy(weight_hbm, weight, weight_sem)
-    fetch.start()
+    for load in loads[:6]:
+        load.wait()
 
     length, channels = x_ref.shape
     groups, states = decay_ref.shape[1:]
@@ -170,6 +151,8 @@
 
     for k in range(1, n_sp):
         hand(k).start()
+    for load in loads[6:9]:
+        load.wait()
     tables = [(table(read_re[k]), table(read_im[k])) for k in range(2)]
     for k in range(1, n_sp):
         arrival(k).wait_recv()
@@ -226,7 +209,8 @@
     for k in range(1, n_tp):
         shift(k, True).start()
     chan[tp] = act[pl.ds(pl.multiple_of(tp * share, share), share), :]
-    fetch.wait()
+    for load in loads[9:]:
+        load.wait()
     for k in range(1, n_tp):
         shift(k, False).wait_recv()
     whole = jnp.concatenate([chan[m] for m in range(n_tp)], axis=1)
@@ -247,14 +231,17 @@
     width = groups * states
     share, model = residual.shape
     flat = lambda a: a.reshape(2, channels, states)
+    operands = (x, log_gate, decay, turn, flat(d_re), flat(d_im), flat(r_re), flat(r_im))
+    operands += (skip[None, :], residual, gain[None, :], weight)
     vmem = pl.BlockSpec(memory_space=pltpu.VMEM)
     dma = pltpu.SemaphoreType.DMA
     return pl.pallas_call(
         functools.partial(mixer_kernel, n_sp, n_tp),
         out_shape=jax.ShapeDtypeStruct((share, model), f32),
-        in_specs=[vmem] * 9 + [pl.BlockSpec(memory_space=pl.ANY)] + [vmem] * 2,
+        in_specs=[pl.BlockSpec(memory_space=pl.ANY)] * len(operands),
         out_specs=vmem,
-        scratch_shapes=[
+        scratch_shapes=[pltpu.VMEM(a.shape, a.dtype) for a in operands]
+        + [
             pltpu.VMEM((4, length, width), f32),
             pltpu.VMEM((length, width), f32),
             pltpu.VMEM((8, segments, width), f32),
@@ -263,31 +250,17 @@
             pltpu.VMEM((n_sp, 8, width), f32),
             pltpu.VMEM((length, channels), bf16),
             pltpu.VMEM((n_tp, share, channels), bf16),
-            pltpu.VMEM(weight.shape, bf16),
-            dma(()),
+            dma((len(operands),)),
             dma((n_sp,)),
             dma((n_sp,)),
             dma((n_tp,)),
             dma((n_tp,)),
         ],
         compiler_params=pltpu.CompilerParams(
-            collective_id=0, has_side_effects=True, vmem_limit_bytes=40 * 2**20
+            collective_id=0, has_side_effects=True, vmem_limit_bytes=60 * 2**20
         ),
         name="mixer",
-    )(
-        x,
-        log_gate,
-        decay,
-        turn,
-        flat(d_re),
-        flat(d_im),
-        flat(r_re),
-        flat(r_im),
-        skip[None, :],
-        weight,
-        residual,
-        gain[None, :],
-    )
+    )(*operands)
 
 
 def experts_kernel(
@@ -346,6 +319,7 @@
     share, model = middle_ref.shape
     length = meta_ref.shape[0]
     slots = rows_out.shape[1]
+    room = -(-slots // 8) * 8
     pick = (iota((length, share), 0) == tp * share + iota((length, share), 1)).astype(f32)
     facts = exact_dot(meta_ref[...], pick, ((0,), (0,)))
     expert = iota((n_sp, share), 0).astype(f32)
@@ -354,7 +328,7 @@
     weights = jnp.where(first, facts[2:3], 0.0) + jnp.where(second, facts[3:4], 0.0)
     before = (iota((share, share), 0) < iota((share, share), 1)).astype(bf16)
     rank = jnp.dot(uses.astype(bf16), before, preferred_element_type=f32)
-    slot = iota((slots, share), 0).astype(f32)
+    slot = iota((room, share), 0).astype(f32)
     chosen = [
         jnp.where(slot == rank[e : e + 1], uses[e : e + 1], 0.0) for e in range(n_sp)
     ]
@@ -362,7 +336,7 @@
     chosen = jnp.concatenate(chosen, axis=0).astype(bf16)
     rows = jnp.dot(chosen, middle_ref[...].astype(bf16), preferred_element_type=f32)
     for e in range(n_sp):
-        rows_out[e] = rows[e * slots : (e + 1) * slots].astype(bf16)
+        rows_out[e] = rows[e * room : e * room + slots].astype(bf16)
 
     pl.semaphore_wait(barrier, n_sp - 1 + n_tp - 1)
 
@@ -420,7 +394,11 @@
         fetch.wait()
 
     def flat(block):
-        return block.astype(f32).reshape(n_sp * slots, model).astype(bf16)
+        block = block.astype(f32)
+        if room > slots:
+            blank = jnp.zeros((n_sp, room - slots, model), f32)
+            block = jnp.concatenate([block, blank], axis=1)
+        return block.reshape(n_sp * room, model).astype(bf16)
 
     def compute(g):
         x = flat(recv[g])
@@ -428,7 +406,7 @@
         b = jnp.dot(x, linear_w[...], preferred_element_type=f32)
         hidden = (jax.nn.silu(a) * b).astype(bf16)
         y = jnp.dot(hidden, down_w[...], preferred_element_type=f32)
-        part[g] = y.reshape(n_sp, slots, model).astype(bf16)
+        part[g] = y.reshape(n_sp, room, model)[:, :slots].astype(bf16)
 
     def give(h):
         go(remote(part.at[h * 2 + 1 - lo], sib.at[h], s3.at[h], r3.at[h], {"tp": sibling}))
@@ -582,7 +560,6 @@
     share = residual.shape[0]
     top = routes.shape[1]
     slots = max(2, 3 * share * top // (2 * experts))
-    slots = -(-slots // 8) * 8
     mixing = group_weight[:, None] * expert_weight / jnp.sum(expert_weight, axis=1, keepdims=True)
     meta = jnp.concatenate([routes.astype(f32), mixing], axis=1)
     return experts_layer(

time: 95.9 us -> 87.5 us (0.912)
  local copies, waits for them, and re-layouts: 13.6 us -> 3.84 us
  Pallas kernels: 79.6 us -> 81.3 us
    unnamed x26 -> x2, local copies, waits for them, and re-layouts: 12.8 us -> 3.07 us
    pallas_call x1, Pallas kernels: 16.4 us -> 18.1 us  [mixer(): pl.pallas_call(functools.partial(mixer_kernel, n_sp, n_tp), out_shape=jax...]
where the time goes in v3:
time: 87.5 us; the launch traced here: 87.3 us
  Pallas kernels  81.3 us (93%)
  local copies, waits for them, and re-layouts  3.84 us (4%)
  other arithmetic  2.1 us (2%)
    pallas_call x1, Pallas kernels, experts_layer(): pl.pallas_call(functools.partial(experts_kernel, n_sp, n_tp), out_shape=j...  63.1 us
    pallas_call x1, Pallas kernels, mixer(): pl.pallas_call(functools.partial(mixer_kernel, n_sp, n_tp), out_shape=jax...  18.1 us
    unnamed x2, local copies, waits for them, and re-layouts  3.07 us

profile of v3, /device:TPU:13, one launch (start us, length us, event | category | flops | bytes accessed | tf_op | source)
XLA Modules:
  0.0 87.3 jit_solution(11728269479849495130)
XLA Ops:
  0.0 0.7 reduce_sum.9
  0.7 0.7 multiply_divide_fusion
  1.4 0.7 convert_element_type.3
  2.1 0.8 copy.26.meta_ref
  2.9 1.5 %copy.25.refs_1_ = f32[192,8]{1,0:T(8,128)} copy(f32[192,8]{0,1:T(8,128)} %param.21) | data formatting | bytes 12288 | tf_op args[2]
  4.3 18.1 %mixer.1.middle_ref = f32[48,2048]{1,0:T(8,128)} custom-call(bf16[192,128]{1,0:T(8,128)(2,1)} %refs_0_.1, f32[192,8]{1,0:T(8,128)} %copy.25.refs_1_, f32[2,8,64]{2,1,0:T(8,128)} %refs_2_.1, f32[2,8,64]{2,1,0:T(8,128)} %refs_3_.1, f32[2,128,64]{2,1,0:T(8,128)} %bitcast.7, f32[2,128,64]{2,1,0:T(8,128)} %bitcast.8, f32[2,128,64]{2,1,0:T(8,128)} %bitcast.9, ...), custom_call_target="tpu_custom_call" | custom-call | tf_op jit(solution)/shard_map/mixer/pallas_call | solution.py:238
  22.5 63.1 %experts.1 = bf16[48,2048]{1,0:T(8,128)(2,1)} custom-call(f32[48,2048]{1,0:T(8,128)} %mixer.1.middle_ref, f32[192,4]{1,0:T(8,128)} %copy.26.meta_ref, f32[1,2048]{1,0:T(1,128)} %bitcast.12, bf16[1,2048,256]{2,1,0:T(8,128)(2,1)} %gate_hbm.1, bf16[1,2048,256]{2,1,0:T(8,128)(2,1)} %linear_hbm.1, bf16[1,256,2048]{2,1,0:T(8,128)(2,1)} %down_hbm.1), custom_call_target="tpu_custom_call" | custom-call | tf_op jit(solution)/shard_map/experts/pallas_call | solution.py:482
  85.6 1.6 %copy.28 = bf16[48,2048]{1,0:T(8,128)(2,1)} copy(bf16[48,2048]{1,0:T(8,128)(2,1)} %experts.1) | data formatting | bytes 393216
  (1 shorter events, 0.0 us)
